TPU v7x, 512 devices: a 4x2x32 block of a 4x8x32 slice. The times are simulated.
512 devices in a mesh: grp: 2 (over y), tp: 32 (over z), dp: 8 (over x, core).
Axes of the slice: x: 4, y: 2, z: 32, core: 2. Of those that a mesh axis runs over, the one named last changes fastest.
The devices are a block of a 4x8x32 slice.
Arguments:
- hidden_in: bfloat16 [192, 4096], P(('grp', 'tp'), 'dp'), parts along dimension 0, may hold values from -40 to 40
- input_norm_gain: float32 [2, 4096], P(None, 'dp'), may hold values from 0.1 to 1.9
- w_query: bfloat16 [2, 4096, 2048], P(None, 'dp', 'tp'), may hold values from -0.09375 to 0.09375
- w_key: bfloat16 [2, 4096, 2048], P(None, 'dp', 'tp'), may hold values from -0.09375 to 0.09375
- w_decay: bfloat16 [2, 4096, 2048], P(None, 'dp', 'tp'), may hold values from -0.375 to 0.375
- w_value: bfloat16 [2, 4096, 4096], P(None, 'dp', 'tp'), may hold values from -0.09375 to 0.09375
- w_gate: bfloat16 [2, 4096, 4096], P(None, 'dp', 'tp'), may hold values from -0.09375 to 0.09375
- out_gain: float32 [2, 4096], P(None, 'tp'), may hold values from 0.1 to 1.9
- w_out: bfloat16 [2, 4096, 4096], P(None, 'tp', 'dp'), may hold values from -0.09375 to 0.09375
- decay_offset: float32 [2, 192, 2048], P(None, ('grp', 'dp'), 'tp'), parts along dimension 1, may hold values from -0.7 to 0
- state: float32 [2, 192, 32, 64, 128], P(None, ('grp', 'dp'), 'tp'), parts along dimension 1, may hold values from -3 to 3
Outputs:
- hidden_out: bfloat16 [192, 4096], P(('grp', 'tp'), 'dp'), parts along dimension 0
- new_state: float32 [2, 192, 32, 64, 128], P(None, ('grp', 'dp'), 'tp'), parts along dimension 1
There are 2 independent parts, one for each index of `grp`. A program takes and returns all parts, laid end to end along the dimension named above; an argument that names none is the same for every part. Nothing has to cross between parts.
All inputs are finite; a program needn't handle non-finite values.
Results may differ from a plain program's by a relative error of at most 0.017.
Values may be sent and summed in bfloat16 or wider, within the bound.
A program may use at most 64 MiB of HBM per device.

v0:
```python
import jax
import jax.numpy as jnp
from jax import lax
from jax.sharding import PartitionSpec as P

D = 4096
HEAD_KEY = 64
VALUE_CHANNELS = 128
LAYERS = 2


epsilon = 1e-06
softness_factor = 16.0


def in_blocks(value, dim, length):
    lengths = value.shape
    blocks = value.reshape(*lengths[:dim], length, lengths[dim] // length, *lengths[dim + 1 :])
    return jnp.moveaxis(blocks, dim, 0)


def summed_on_arrival(value, axis, dim):
    blocks = in_blocks(value, dim, lax.axis_size(axis))
    arrived = lax.all_to_all(blocks, axis, split_axis=0, concat_axis=0, tiled=True)
    return arrived.astype(jnp.float32).sum(axis=0)


def copy_for_each(value, axis):
    length = lax.axis_size(axis)
    return lax.all_to_all(
        jnp.broadcast_to(value[None], (length, *value.shape)), axis, 0, 0, tiled=True
    )


def joined_along(blocks, dim):
    lengths = list(blocks.shape[1:])
    lengths[dim] *= blocks.shape[0]
    return jnp.moveaxis(blocks, 0, dim).reshape(lengths)


def gathered_copies(value, axis, dim):
    blocks = copy_for_each(value, axis)
    return joined_along(blocks, dim)


def of_everyone(value, axis):
    everything = copy_for_each(value, axis)
    return jnp.sum(everything, axis=0)


def split_heads_sum(head_terms, current):
    own_part = summed_on_arrival(head_terms.astype(jnp.bfloat16), "tp", 0)
    return (current.astype(jnp.float32) + own_part).astype(jnp.bfloat16)


def per_device(
    hidden_in,
    input_norm_gain,
    w_query,
    w_key,
    w_decay,
    w_value,
    w_gate,
    out_gain,
    w_out,
    decay_offset,
    state,
):
    seq_rows = state.shape[1]
    local_heads = state.shape[2]
    key_cols = local_heads * HEAD_KEY
    value_cols = local_heads * VALUE_CHANNELS
    seq_start = lax.axis_index("dp") * seq_rows
    current = hidden_in
    gathered = None
    states = []
    for index_of_block in range(LAYERS):
        gathered = gathered_copies(current, "tp", 0)
        widened = gathered.astype(jnp.float32)
        squares = jnp.sum(widened * widened, axis=1)
        scaled_query = (widened * input_norm_gain[index_of_block][None, :]).astype(jnp.bfloat16)
        partial_value = jnp.concatenate(
            [
                jnp.dot(scaled_query, matrix[index_of_block], preferred_element_type=jnp.float32)
                for matrix in (w_query, w_key, w_decay, w_value, w_gate)
            ],
            axis=1,
        ).astype(jnp.bfloat16)
        summed = summed_on_arrival(partial_value, "dp", 0)
        whole_squares = of_everyone(squares, "dp")
        own_squares = lax.dynamic_slice_in_dim(whole_squares, seq_start, seq_rows)
        inverse = lax.rsqrt(own_squares / D + epsilon)[:, None]
        projected = summed * inverse
        query_rows = projected[:, :key_cols].reshape(seq_rows, local_heads, HEAD_KEY)
        key_rows = projected[:, key_cols : 2 * key_cols].reshape(
            seq_rows, local_heads, HEAD_KEY
        ) * HEAD_KEY ** (-0.5)
        decay_logits = projected[:, 2 * key_cols : 3 * key_cols]
        value_rows = projected[:, 3 * key_cols : 3 * key_cols + value_cols].reshape(
            seq_rows, local_heads, VALUE_CHANNELS
        )
        gate_rows = projected[:, 3 * key_cols + value_cols :].reshape(
            seq_rows, local_heads, VALUE_CHANNELS
        )
        decay_logarithm = (
            jax.nn.log_sigmoid(decay_logits) / softness_factor + decay_offset[index_of_block]
        )
        decay_rate = jnp.exp(decay_logarithm).reshape(seq_rows, local_heads, HEAD_KEY)
        fresh = (
            decay_rate[:, :, :, None] * state[index_of_block]
            + key_rows[:, :, :, None] * value_rows[:, :, None, :]
        )
        readout = jnp.sum(query_rows[:, :, :, None] * fresh, axis=2)
        normed = readout * lax.rsqrt(jnp.mean(readout * readout, axis=2, keepdims=True) + epsilon)
        normed = normed * out_gain[index_of_block].reshape(local_heads, VALUE_CHANNELS)[None]
        gated_out = (
            (normed * jax.nn.silu(gate_rows)).reshape(seq_rows, value_cols).astype(jnp.bfloat16)
        )
        out_matrix = w_out[index_of_block]
        head_terms = jnp.dot(
            gathered_copies(gated_out, "dp", 0), out_matrix, preferred_element_type=jnp.float32
        )
        current = split_heads_sum(head_terms, current)
        gathered = None
        states.append(fresh)
    return (current, jnp.stack(states))


def solution(mesh):
    return jax.shard_map(
        per_device,
        mesh=mesh,
        in_specs=(
            P(("grp", "tp"), "dp"),
            P(None, "dp"),
            P(None, "dp", "tp"),
            P(None, "dp", "tp"),
            P(None, "dp", "tp"),
            P(None, "dp", "tp"),
            P(None, "dp", "tp"),
            P(None, "tp"),
            P(None, "tp", "dp"),
            P(None, ("grp", "dp"), "tp"),
            P(None, ("grp", "dp"), "tp", None, None),
        ),
        out_specs=(P(("grp", "tp"), "dp"), P(None, ("grp", "dp"), "tp", None, None)),
        check_vma=False,
    )
```

profile of v0, /device:TPU:33, one launch (start us, length us, event | category | flops | bytes accessed | tf_op | source)
XLA Modules:
  0.0 241.0 jit_solution(2516870819133110794)
XLA Ops:
  0.6 1.4 broadcast_in_dim.16
  2.0 46.4 %all-to-all-start = ((bf16[32,3,512]{2,1,0:T(4,128)(2,1)}), bf16[32,3,512]{2,1,0:T(4,128)(2,1)S(1)}, u32[]{:S(2)}, u32[]{:S(2)}) async-start(bf16[32,3,512]{2,1,0:T(4,128)(2,1)} %broadcast_in_dim.16), calls=%async_computation | async-start | bytes 262144 | tf_op jit(solution)/shard_map/all_to_all | solution.py:30
  48.5 0.7 copy-done.10
  49.2 28.3 %all-to-all-done = bf16[32,3,512]{2,1,0:T(4,128)(2,1)S(1)} async-done(((bf16[32,3,512]{2,1,0:T(4,128)(2,1)}), bf16[32,3,512]{2,1,0:T(4,128)(2,1)S(1)}, u32[]{:S(2)}, u32[]{:S(2)}) %all-to-all-start) | async-done | bytes 98336 | tf_op jit(solution)/shard_map/all_to_all | solution.py:30
  77.8 0.6 broadcast_in_dim.18
  78.4 7.3 %all-to-all-start.2 = ((f32[8,1,96]{2,1,0:T(1,128)}), f32[8,1,96]{2,1,0:T(1,128)S(1)}, u32[]{:S(2)}, u32[]{:S(2)}) async-start(f32[8,1,96]{2,1,0:T(1,128)} %broadcast_in_dim.18), calls=%async_computation.2 | async-start | bytes 8192 | tf_op jit(solution)/shard_map/all_to_all | solution.py:30
  86.0 0.7 copy-done.2
  86.9 0.7 copy-done.4
  88.1 0.8 concatenate.10
  88.9 1.3 all-to-all-done.2
  90.2 4.0 %all-to-all-start.1 = ((bf16[8,12,448]{2,1,0:T(8,128)(2,1)}), bf16[8,12,448]{2,1,0:T(8,128)(2,1)S(1)}, u32[]{:S(2)}, u32[]{:S(2)}) async-start(bf16[8,12,448]{2,1,0:T(8,128)(2,1)} %concatenate.10), calls=%async_computation.1 | async-start | bytes 262144 | tf_op jit(solution)/shard_map/all_to_all | solution.py:24
  94.3 5.2 %all-to-all-done.1 = bf16[8,12,448]{2,1,0:T(8,128)(2,1)S(1)} async-done(((bf16[8,12,448]{2,1,0:T(8,128)(2,1)}), bf16[8,12,448]{2,1,0:T(8,128)(2,1)S(1)}, u32[]{:S(2)}, u32[]{:S(2)}) %all-to-all-start.1) | async-done | bytes 86048 | tf_op jit(solution)/shard_map/all_to_all | solution.py:24
  99.8 0.4 fusion.5
  100.4 8.0 %all_to_all.52 = bf16[8,12,128]{2,1,0:T(8,128)(2,1)S(1)} all-to-all(bf16[8,12,128]{2,1,0:T(8,128)(2,1)S(1)} %broadcast_in_dim.19), channel_id=1, replica_groups=mesh['grp'=2,'tp'=32,'dp'=8] {'dp'}, dimensions={0} | all-to-all | bytes 49152 | tf_op jit(solution)/shard_map/all_to_all | solution.py:30
  108.7 32.5 %all_to_all.53 = bf16[32,3,512]{2,1,0:T(4,128)(2,1)S(1)} all-to-all(bf16[32,3,512]{2,1,0:T(4,128)(2,1)S(1)} %reshape.295), channel_id=1, replica_groups=mesh['grp'=2,'tp'=32,'dp'=8] {'tp'}, dimensions={0} | all-to-all | bytes 196608 | tf_op jit(solution)/shard_map/all_to_all | solution.py:24
  141.3 0.6 copy-done.7
  141.9 31.9 %all_to_all.54 = bf16[32,3,512]{2,1,0:T(4,128)(2,1)S(1)} all-to-all(bf16[32,3,512]{2,1,0:T(4,128)(2,1)S(1)} %broadcast_in_dim.20), channel_id=1, replica_groups=mesh['grp'=2,'tp'=32,'dp'=8] {'tp'}, dimensions={0} | all-to-all | bytes 196608 | tf_op jit(solution)/shard_map/all_to_all | solution.py:30
  173.8 0.2 fusion.9
  174.9 0.6 broadcast_in_dim.22
  175.5 7.7 %all-to-all-start.7 = ((f32[8,1,96]{2,1,0:T(1,128)}), f32[8,1,96]{2,1,0:T(1,128)S(1)}, u32[]{:S(2)}, u32[]{:S(2)}) async-start(f32[8,1,96]{2,1,0:T(1,128)} %broadcast_in_dim.22), calls=%async_computation.7 | async-start | bytes 8192 | tf_op jit(solution)/shard_map/all_to_all | solution.py:30
  183.4 0.8 concatenate.11
  184.2 3.6 %all-to-all-done.7 = f32[8,1,96]{2,1,0:T(1,128)S(1)} async-done(((f32[8,1,96]{2,1,0:T(1,128)}), f32[8,1,96]{2,1,0:T(1,128)S(1)}, u32[]{:S(2)}, u32[]{:S(2)}) %all-to-all-start.7) | async-done | bytes 3104 | tf_op jit(solution)/shard_map/all_to_all | solution.py:30
  187.8 4.0 %all-to-all-start.6 = ((bf16[8,12,448]{2,1,0:T(8,128)(2,1)}), bf16[8,12,448]{2,1,0:T(8,128)(2,1)S(1)}, u32[]{:S(2)}, u32[]{:S(2)}) async-start(bf16[8,12,448]{2,1,0:T(8,128)(2,1)} %concatenate.11), calls=%async_computation.6 | async-start | bytes 262144 | tf_op jit(solution)/shard_map/all_to_all | solution.py:24
  191.9 5.2 %all-to-all-done.6 = bf16[8,12,448]{2,1,0:T(8,128)(2,1)S(1)} async-done(((bf16[8,12,448]{2,1,0:T(8,128)(2,1)}), bf16[8,12,448]{2,1,0:T(8,128)(2,1)S(1)}, u32[]{:S(2)}, u32[]{:S(2)}) %all-to-all-start.6) | async-done | bytes 86048 | tf_op jit(solution)/shard_map/all_to_all | solution.py:24
  197.4 0.4 fusion.2
  198.0 8.0 %all_to_all.55 = bf16[8,12,128]{2,1,0:T(8,128)(2,1)S(1)} all-to-all(bf16[8,12,128]{2,1,0:T(8,128)(2,1)S(1)} %broadcast_in_dim.23), channel_id=1, replica_groups=mesh['grp'=2,'tp'=32,'dp'=8] {'dp'}, dimensions={0} | all-to-all | bytes 49152 | tf_op jit(solution)/shard_map/all_to_all | solution.py:30
  206.2 0.7 reshape.297
  206.9 4.8 %all-to-all-start.9 = ((bf16[32,3,512]{2,1,0:T(4,128)(2,1)}), bf16[32,3,512]{2,1,0:T(4,128)(2,1)S(1)}, u32[]{:S(2)}, u32[]{:S(2)}) async-start(bf16[32,3,512]{2,1,0:T(4,128)(2,1)} %reshape.297), calls=%async_computation.9 | async-start | bytes 262144 | tf_op jit(solution)/shard_map/all_to_all | solution.py:24
  211.7 0.5 multiply_add_fusion.1
  212.2 0.9 pad_maximum_fusion
  213.1 27.2 %all-to-all-done.9 = bf16[32,3,512]{2,1,0:T(4,128)(2,1)S(1)} async-done(((bf16[32,3,512]{2,1,0:T(4,128)(2,1)}), bf16[32,3,512]{2,1,0:T(4,128)(2,1)S(1)}, u32[]{:S(2)}, u32[]{:S(2)}) %all-to-all-start.9) | async-done | bytes 98336 | tf_op jit(solution)/shard_map/all_to_all | solution.py:24
  240.4 0.6 add_convert_fusion
  (65 shorter events, 4.0 us)
Async XLA Ops:
  2.0 47.1 %copy-start.9 = (f32[2,512]{1,0:T(2,128)S(1)}, f32[2,512]{1,0:T(2,128)}, u32[]{:S(2)}) copy-start(f32[2,512]{1,0:T(2,128)} %param.12) | copy-start | bytes 12292
  2.0 75.5 %all-to-all-start = ((bf16[32,3,512]{2,1,0:T(4,128)(2,1)}), bf16[32,3,512]{2,1,0:T(4,128)(2,1)S(1)}, u32[]{:S(2)}, u32[]{:S(2)}) async-start(bf16[32,3,512]{2,1,0:T(4,128)(2,1)} %broadcast_in_dim.16), calls=%async_computation | async-start | bytes 262144 | tf_op jit(solution)/shard_map/all_to_all | solution.py:30
  48.5 0.7 copy-start.8
  48.5 0.7 copy-start.10
  77.5 8.3 %copy-start.1 = (bf16[2,512,128]{2,1,0:T(8,128)(2,1)S(1)}, bf16[2,512,128]{2,1,0:T(8,128)(2,1)}, u32[]{:S(2)}) copy-start(bf16[2,512,128]{2,1,0:T(8,128)(2,1)} %param.17) | copy-start | bytes 786436
  78.4 11.9 %all-to-all-start.2 = ((f32[8,1,96]{2,1,0:T(1,128)}), f32[8,1,96]{2,1,0:T(1,128)S(1)}, u32[]{:S(2)}, u32[]{:S(2)}) async-start(f32[8,1,96]{2,1,0:T(1,128)} %broadcast_in_dim.18), calls=%async_computation.2 | async-start | bytes 8192 | tf_op jit(solution)/shard_map/all_to_all | solution.py:30
  85.7 0.9 copy-start.2
  86.7 0.9 copy-start.4
  86.7 1.1 copy-start.5
  86.7 1.3 copy-start.6
  87.6 12.2 %copy-start = (f32[2,12,1,64,128]{4,3,2,1,0:T(8,128)S(1)}, f32[2,12,1,64,128]{4,3,2,1,0:T(8,128)}, u32[]{:S(2)}) copy-start(f32[2,12,1,64,128]{4,3,2,1,0:T(8,128)} %param.21) | copy-start | bytes 2359300
  90.2 9.3 %all-to-all-start.1 = ((bf16[8,12,448]{2,1,0:T(8,128)(2,1)}), bf16[8,12,448]{2,1,0:T(8,128)(2,1)S(1)}, u32[]{:S(2)}, u32[]{:S(2)}) async-start(bf16[8,12,448]{2,1,0:T(8,128)(2,1)} %concatenate.10), calls=%async_computation.1 | async-start | bytes 262144 | tf_op jit(solution)/shard_map/all_to_all | solution.py:24
  99.8 8.7 %copy-start.3 = (bf16[2,128,512]{2,1,0:T(8,128)(2,1)S(1)}, bf16[2,128,512]{2,1,0:T(8,128)(2,1)}, u32[]{:S(2)}) copy-start(bf16[2,128,512]{2,1,0:T(8,128)(2,1)} %param.19) | copy-start | bytes 786436
  141.2 0.7 copy-start.7
  175.5 12.3 %all-to-all-start.7 = ((f32[8,1,96]{2,1,0:T(1,128)}), f32[8,1,96]{2,1,0:T(1,128)S(1)}, u32[]{:S(2)}, u32[]{:S(2)}) async-start(f32[8,1,96]{2,1,0:T(1,128)} %broadcast_in_dim.22), calls=%async_computation.7 | async-start | bytes 8192 | tf_op jit(solution)/shard_map/all_to_all | solution.py:30
  187.8 9.3 %all-to-all-start.6 = ((bf16[8,12,448]{2,1,0:T(8,128)(2,1)}), bf16[8,12,448]{2,1,0:T(8,128)(2,1)S(1)}, u32[]{:S(2)}, u32[]{:S(2)}) async-start(bf16[8,12,448]{2,1,0:T(8,128)(2,1)} %concatenate.11), calls=%async_computation.6 | async-start | bytes 262144 | tf_op jit(solution)/shard_map/all_to_all | solution.py:24
  206.9 33.4 %all-to-all-start.9 = ((bf16[32,3,512]{2,1,0:T(4,128)(2,1)}), bf16[32,3,512]{2,1,0:T(4,128)(2,1)S(1)}, u32[]{:S(2)}, u32[]{:S(2)}) async-start(bf16[32,3,512]{2,1,0:T(4,128)(2,1)} %reshape.297), calls=%async_computation.9 | async-start | bytes 262144 | tf_op jit(solution)/shard_map/all_to_all | solution.py:24
where the time goes:
time: 244 us; the launch traced here: 241 us
  blocking collectives  80.4 us (33%)
  starting transfers between devices  74.2 us (30%)
  waiting for transfers between devices  70.9 us (29%)
  local copies, waits for them, and re-layouts  8.26 us (3%)
  other arithmetic  4.26 us (2%)
    all_to_all x3, starting transfers between devices, copy_for_each(): lax.all_to_all(jnp.broadcast_to(value[None], (length, *value.shape)), axi...  61.5 us
    all_to_all x3, blocking collectives, copy_for_each(): lax.all_to_all(jnp.broadcast_to(value[None], (length, *value.shape)), axi...  47.9 us
    all_to_all x3, waiting for transfers between devices, summed_on_arrival(): lax.all_to_all(blocks, axis, split_axis=0, concat_axis=0, tiled=True)  37.6 us
    all_to_all x3, waiting for transfers between devices, copy_for_each(): lax.all_to_all(jnp.broadcast_to(value[None], (length, *value.shape)), axi...  33.3 us
    all_to_all x1, blocking collectives, summed_on_arrival(): lax.all_to_all(blocks, axis, split_axis=0, concat_axis=0, tiled=True)  32.5 us
    all_to_all x3, starting transfers between devices, summed_on_arrival(): lax.all_to_all(blocks, axis, split_axis=0, concat_axis=0, tiled=True)  12.7 us
  transfers between devices with their start and end apart: 6, of which 6 were waited for; matrix products, arithmetic and copies ran while one was open for 2% of the time, Pallas kernels for 0%

commit v1 on v0

v1 whole, which is shorter than its diff:
```python
import functools

import jax
import jax.numpy as jnp
from jax import lax
from jax.experimental import pallas as pl
from jax.experimental.pallas import tpu as pltpu
from jax.sharding import PartitionSpec as P

D = 4096
HEAD_KEY = 64
VALUE_CHANNELS = 128
LAYERS = 2

epsilon = 1e-06
softness_factor = 16.0

MESH = pl.DeviceIdType.MESH


def kernel(
    n_tp,
    n_dp,
    hidden,
    gain,
    w_query,
    w_key,
    w_decay,
    w_value,
    w_gate,
    out_gain,
    w_out,
    decay_offset,
    state,
    hidden_out,
    new_state,
    h_v,
    gain_v,
    qkd_v,
    wcat,
    ogain_v,
    wout_v,
    off_v,
    st,
    ag,
    part_send,
    part_recv,
    gat,
    rs_send,
    rs_recv,
    xs,
    pk,
    local_sem,
    state_sem,
    out_sem,
    ag_send_sem,
    ag_sem,
    part_send_sem,
    part_sem,
    gat_send_sem,
    gat_sem,
    rs_send_sem,
    rs_sem,
):
    rows, feats = h_v.shape
    half = feats // 2
    members = n_tp // n_dp
    seqs = rows * members
    p = lax.axis_index("tp")
    d = lax.axis_index("dp")
    group = p // members
    place = p % members
    anti = (p + n_tp // 2) % n_tp
    near_first = jnp.where(2 * place >= members, 1, -1)

    barrier = pltpu.get_barrier_semaphore()

    def greet_tp(i, c):
        pl.semaphore_signal(
            barrier, inc=1, device_id={"tp": (p + 1 + i) % n_tp}, device_id_type=MESH
        )
        return c

    def greet_dp(i, c):
        pl.semaphore_signal(
            barrier, inc=1, device_id={"dp": (d + 1 + i) % n_dp}, device_id_type=MESH
        )
        return c

    lax.fori_loop(0, n_tp - 1, greet_tp, 0)
    lax.fori_loop(0, n_dp - 1, greet_dp, 0)

    fetches = [
        pltpu.make_async_copy(hidden, h_v, local_sem.at[0]),
        pltpu.make_async_copy(gain, gain_v, local_sem.at[1]),
        pltpu.make_async_copy(w_query, qkd_v.at[0], local_sem.at[2]),
        pltpu.make_async_copy(w_key, qkd_v.at[1], local_sem.at[3]),
        pltpu.make_async_copy(w_decay, qkd_v.at[2], local_sem.at[4]),
        pltpu.make_async_copy(w_value, wcat.at[:, :, pl.ds(256, 128)], local_sem.at[5]),
        pltpu.make_async_copy(w_gate, wcat.at[:, :, pl.ds(384, 128)], local_sem.at[6]),
        pltpu.make_async_copy(out_gain, ogain_v, local_sem.at[7]),
        pltpu.make_async_copy(w_out, wout_v, local_sem.at[8]),
        pltpu.make_async_copy(decay_offset, off_v, local_sem.at[9]),
    ]
    for f in fetches:
        f.start()
    state_in = [
        pltpu.make_async_copy(state.at[l, :, 0], st.at[l], state_sem.at[l]) for l in range(LAYERS)
    ]
    for f in state_in:
        f.start()
    for f in fetches:
        f.wait()

    xs[...] = jnp.zeros_like(xs)

    first = h_v[...].astype(jnp.float32)
    pk[0, 0:1, 0:feats] = first[0:1]
    pk[0, 0:1, feats : feats + half] = first[1:2, 0:half]
    pk[0, 1:2, 0:half] = first[1:2, half:feats]
    pk[0, 1:2, half : half + feats] = first[2:3]
    ag[0, p] = pk[0].astype(jnp.bfloat16)

    for l in range(LAYERS):
        wcat[l, :, 0:128] = jnp.concatenate([qkd_v[0, l], qkd_v[1, l]], axis=-1)
        wcat[l, :, 128:256] = jnp.concatenate(
            [qkd_v[2, l], jnp.zeros_like(qkd_v[2, l])], axis=-1
        )

    pl.semaphore_wait(barrier, n_tp - 1 + n_dp - 1)

    def source_group(i):
        k = (i + 1) // 2
        side = jnp.where(i % 2 == 1, near_first, -near_first)
        return (group + n_dp + side * k) % n_dp

    def row_group(l, i):
        return (source_group(i) + l * (n_dp // 2)) % n_dp

    def gather_copy(l, peer):
        return pltpu.make_async_remote_copy(
            src_ref=ag.at[l, p],
            dst_ref=ag.at[l, p],
            send_sem=ag_send_sem.at[l],
            recv_sem=ag_sem.at[l, group],
            device_id={"tp": peer},
            device_id_type=MESH,
        )

    def gather_start(l):
        def one(i, c):
            k = n_tp // 2 - (i + 1) // 2
            off = jnp.where(i % 2 == 1, k, n_tp - k)
            gather_copy(l, (p + off) % n_tp).start()
            return c

        lax.fori_loop(0, n_tp - 1, one, 0)

    def gather_wait(l, sg, first_slot, count):
        block = ag.at[l, pl.ds(first_slot, count)]
        pltpu.make_async_remote_copy(
            src_ref=block,
            dst_ref=block,
            send_sem=ag_send_sem.at[l],
            recv_sem=ag_sem.at[l, sg],
            device_id={"tp": anti},
            device_id_type=MESH,
        ).wait_recv()

    def part_copy(l, i, to):
        slot = (d - to + n_dp) % n_dp - 1
        return pltpu.make_async_remote_copy(
            src_ref=part_send.at[l, i],
            dst_ref=part_recv.at[l, slot],
            send_sem=part_send_sem.at[l],
            recv_sem=part_sem.at[l],
            device_id={"dp": to},
            device_id_type=MESH,
        )

    lane = lax.broadcasted_iota(jnp.int32, (seqs, 512), 1)

    def project(l, i):
        sg = source_group(i)
        for j in range(members):
            b = ag[l, sg * members + j].astype(jnp.float32)
            xs[3 * j : 3 * j + 1, :] = b[0:1, 0:feats]
            xs[3 * j + 1 : 3 * j + 2, 0:half] = b[0:1, feats : feats + half]
            xs[3 * j + 1 : 3 * j + 2, half:feats] = b[1:2, 0:half]
            xs[3 * j + 2 : 3 * j + 3, :] = b[1:2, half : half + feats]
        x = xs[...]
        squares = jnp.sum(x * x, axis=1, keepdims=True)[0:seqs]
        scaled = (x * gain_v[l : l + 1, :]).astype(jnp.bfloat16)
        y = jnp.dot(scaled, wcat[l], preferred_element_type=jnp.float32)[0:seqs]
        high = squares.astype(jnp.bfloat16).astype(jnp.float32)
        rest = squares - high
        mid = rest.astype(jnp.bfloat16).astype(jnp.float32)
        low = rest - mid
        y = jnp.where(lane == 192, high, y)
        y = jnp.where(lane == 193, mid, y)
        y = jnp.where(lane == 194, low, y)
        part_send[l, i] = y.astype(jnp.bfloat16)
        to = row_group(l, i)

        @pl.when(to != d)
        def _():
            part_copy(l, i, to).start()

    def gat_copy(l, i, peer):
        return pltpu.make_async_remote_copy(
            src_ref=gat.at[l, i],
            dst_ref=gat.at[l, i],
            send_sem=gat_send_sem.at[l],
            recv_sem=gat_sem.at[l, i],
            device_id={"dp": peer},
            device_id_type=MESH,
        )

    def update(l, i):
        @pl.when(row_group(l, i) == d)
        def _():
            pltpu.make_async_remote_copy(
                src_ref=part_recv.at[l],
                dst_ref=part_recv.at[l],
                send_sem=part_send_sem.at[l],
                recv_sem=part_sem.at[l],
                device_id={"tp": anti},
                device_id_type=MESH,
            ).wait_recv()
            total = part_send[l, i].astype(jnp.float32)
            for k in range(n_dp - 1):
                total += part_recv[l, k].astype(jnp.float32)
            squares = jnp.sum(total[:, 192:195], axis=1, keepdims=True)
            projected = total * lax.rsqrt(squares / D + epsilon)
            query_key = projected[:, 0:128]
            decay_pre = projected[:, 128:256]
            value = projected[:, 256:384]
            gate = projected[:, 384:512]
            log_sig = jnp.minimum(decay_pre, 0.0) - jnp.log1p(jnp.exp(-jnp.abs(decay_pre)))
            rate = jnp.exp(log_sig[:, 0:HEAD_KEY] / softness_factor + off_v[l])
            columns_qk = jnp.transpose(query_key, (1, 0))
            columns_rate = jnp.transpose(jnp.concatenate([rate, rate], axis=1), (1, 0))
            outs = []
            for s in range(seqs):
                q = columns_qk[0:HEAD_KEY, s : s + 1]
                k = columns_qk[HEAD_KEY : 2 * HEAD_KEY, s : s + 1] * HEAD_KEY ** (-0.5)
                r = columns_rate[0:HEAD_KEY, s : s + 1]
                fresh = r * st[l, s] + k * value[s : s + 1, :]
                st[l, s] = fresh
                outs.append(jnp.sum(q * fresh, axis=0, keepdims=True))
            readout = jnp.concatenate(outs, axis=0)
            normed = readout * lax.rsqrt(
                jnp.mean(readout * readout, axis=1, keepdims=True) + epsilon
            )
            normed = normed * ogain_v[l : l + 1, :]
            silu = gate / (1.0 + jnp.exp(-gate))
            gat[l, i] = (normed * silu).astype(jnp.bfloat16)

            def send(j, c):
                gat_copy(l, i, (d + 1 + j) % n_dp).start()
                return c

            lax.fori_loop(0, n_dp - 1, send, 0)
            pltpu.make_async_copy(st.at[l], new_state.at[l, :, 0], out_sem.at[l]).start()

    def reduce_copy(l, slot, owner):
        return pltpu.make_async_remote_copy(
            src_ref=rs_send.at[l, slot],
            dst_ref=rs_recv.at[l, (p - owner + n_tp) % n_tp - 1],
            send_sem=rs_send_sem.at[l],
            recv_sem=rs_sem.at[l],
            device_id={"tp": owner},
            device_id_type=MESH,
        )

    def out_project(l, i):
        @pl.when(row_group(l, i) != d)
        def _():
            gat_copy(l, i, row_group(l, i)).wait_recv()

        y = jnp.dot(gat[l, i], wout_v[l], preferred_element_type=jnp.float32)
        for j in range(members):
            pk[j, 0:1, 0:feats] = y[3 * j : 3 * j + 1]
            pk[j, 0:1, feats : feats + half] = y[3 * j + 1 : 3 * j + 2, 0:half]
            pk[j, 1:2, 0:half] = y[3 * j + 1 : 3 * j + 2, half:feats]
            pk[j, 1:2, half : half + feats] = y[3 * j + 2 : 3 * j + 3]
        base = source_group(i) * members + n_tp // 2
        for j in range(members):
            slot = members * i + j
            rs_send[l, slot] = pk[j].astype(jnp.bfloat16)
        for j in range(members):
            slot = members * i + j
            owner = (base + j) % n_tp

            @pl.when(owner != p)
            def _():
                reduce_copy(l, slot, owner).start()

    def loop(start, stop, fn):
        def step(i, c):
            fn(i)
            return c

        lax.fori_loop(start, stop, step, 0)

    lead = n_dp // 2
    for l in range(LAYERS):
        gather_start(l)

        def arrive(i):
            sg = source_group(i)
            gather_wait(l, sg, sg * members, members)
            project(l, i)

        gather_wait(l, group, 0, members - 1)
        project(l, 0)
        loop(1, lead, arrive)
        state_in[l].wait()

        def early(i):
            update(l, i)
            arrive(i + lead)

        def late(i):
            out_project(l, i)
            update(l, i + lead)

        loop(0, lead, early)
        loop(0, lead, late)
        loop(lead, n_dp, lambda i: out_project(l, i))

        pltpu.make_async_remote_copy(
            src_ref=rs_recv.at[l],
            dst_ref=rs_recv.at[l],
            send_sem=rs_send_sem.at[l],
            recv_sem=rs_sem.at[l],
            device_id={"tp": anti},
            device_id_type=MESH,
        ).wait_recv()
        total = rs_send[l, members * (n_dp - 1) + place].astype(jnp.float32)
        total += jnp.sum(rs_recv[l].astype(jnp.float32), axis=0)
        result = (total + ag[l, anti].astype(jnp.float32)).astype(jnp.bfloat16)
        if l + 1 < LAYERS:
            ag[l + 1, p] = result
        else:
            b = result.astype(jnp.float32)
            xs[0:1, :] = b[0:1, 0:feats]
            xs[1:2, 0:half] = b[0:1, feats : feats + half]
            xs[1:2, half:feats] = b[1:2, 0:half]
            xs[2:3, :] = b[1:2, half : half + feats]
            hidden_out[...] = xs[0:rows, :].astype(jnp.bfloat16)

    for l in range(LAYERS):
        for buf, sem, count in (
            (rs_recv, rs_send_sem, n_tp - 1),
            (part_recv, part_send_sem, n_dp - 1),
        ):
            ref = buf.at[l]
            pltpu.make_async_remote_copy(
                src_ref=ref, dst_ref=ref, send_sem=sem.at[l], recv_sem=rs_sem.at[l],
                device_id={"tp": anti}, device_id_type=MESH,
            ).wait_send()
        for buf, sem, count in (
            (ag, ag_send_sem, n_tp - 1),
            (gat, gat_send_sem, n_dp - 1),
        ):
            ref = buf.at[l, pl.ds(0, count)]
            pltpu.make_async_remote_copy(
                src_ref=ref, dst_ref=ref, send_sem=sem.at[l], recv_sem=rs_sem.at[l],
                device_id={"tp": anti}, device_id_type=MESH,
            ).wait_send()
        pltpu.make_async_copy(st.at[l], new_state.at[l, :, 0], out_sem.at[l]).wait()


def per_device(n_tp, n_dp, *args):
    hidden, state = args[0], args[10]
    rows, feats = hidden.shape
    members = n_tp // n_dp
    seqs = state.shape[1]
    block = (2, rows * feats // 2)
    any_spec = pl.BlockSpec(memory_space=pl.ANY)
    bf16, f32 = jnp.bfloat16, jnp.float32
    cols = 512
    dma = pltpu.SemaphoreType.DMA
    return pl.pallas_call(
        functools.partial(kernel, n_tp, n_dp),
        name="decode",
        out_shape=(
            jax.ShapeDtypeStruct(hidden.shape, hidden.dtype),
            jax.ShapeDtypeStruct(state.shape, state.dtype),
        ),
        in_specs=[any_spec] * 11,
        out_specs=(pl.BlockSpec(memory_space=pltpu.VMEM), any_spec),
        scratch_shapes=[
            pltpu.VMEM(hidden.shape, bf16),
            pltpu.VMEM(args[1].shape, f32),
            pltpu.VMEM((3,) + args[2].shape, bf16),
            pltpu.VMEM((LAYERS, feats, cols), bf16),
            pltpu.VMEM(args[7].shape, f32),
            pltpu.VMEM(args[8].shape, bf16),
            pltpu.VMEM(args[9].shape, f32),
            pltpu.VMEM((LAYERS, seqs) + state.shape[3:], f32),
            pltpu.VMEM((LAYERS, n_tp) + block, bf16),
            pltpu.VMEM((LAYERS, n_dp, seqs, cols), bf16),
            pltpu.VMEM((LAYERS, n_dp - 1, seqs, cols), bf16),
            pltpu.VMEM((LAYERS, n_dp, seqs, VALUE_CHANNELS), bf16),
            pltpu.VMEM((LAYERS, n_tp) + block, bf16),
            pltpu.VMEM((LAYERS, n_tp - 1) + block, bf16),
            pltpu.VMEM((16, feats), f32),
            pltpu.VMEM((members,) + block, f32),
            dma((10,)),
            dma((LAYERS,)),
            dma((LAYERS,)),
            dma((LAYERS,)),
            dma((LAYERS, n_dp)),
            dma((LAYERS,)),
            dma((LAYERS,)),
            dma((LAYERS,)),
            dma((LAYERS, n_dp)),
            dma((LAYERS,)),
            dma((LAYERS,)),
        ],
        compiler_params=pltpu.CompilerParams(
            collective_id=0, has_side_effects=True, vmem_limit_bytes=32 * 1024 * 1024
        ),
    )(*args)


def solution(mesh):
    return jax.shard_map(
        functools.partial(per_device, mesh.shape["tp"], mesh.shape["dp"]),
        mesh=mesh,
        in_specs=(
            P(("grp", "tp"), "dp"),
            P(None, "dp"),
            P(None, "dp", "tp"),
            P(None, "dp", "tp"),
            P(None, "dp", "tp"),
            P(None, "dp", "tp"),
            P(None, "dp", "tp"),
            P(None, "tp"),
            P(None, "tp", "dp"),
            P(None, ("grp", "dp"), "tp"),
            P(None, ("grp", "dp"), "tp", None, None),
        ),
        out_specs=(P(("grp", "tp"), "dp"), P(None, ("grp", "dp"), "tp", None, None)),
        check_vma=False,
    )
```

time: 244 us -> 128 us (0.52)
  Pallas kernels: 0 us -> 119 us
  blocking collectives: 80.4 us -> 0 us
  starting transfers between devices: 74.2 us -> 0 us
  waiting for transfers between devices: 70.9 us -> 0 us
  other arithmetic: 4.26 us -> 0 us
    pallas_call x0 -> x1, Pallas kernels: none -> 119 us  [per_device(): pl.pallas_call(functools.partial(kernel, n_tp, n_dp), name='decode', out_...]
    all_to_all x4 -> x0, blocking collectives: 80.4 us -> none  [the longest x3 47.9 us: copy_for_each(): lax.all_to_all(jnp.broadcast_to(value[None], (length, *value.shape)), axi...]
    all_to_all x6 -> x0, starting transfers between devices: 74.2 us -> none  [the longest x3 61.5 us: copy_for_each(): lax.all_to_all(jnp.broadcast_to(value[None], (length, *value.shape)), axi...]
    all_to_all x6 -> x0, waiting for transfers between devices: 70.9 us -> none  [the longest x3 37.6 us: summed_on_arrival(): lax.all_to_all(blocks, axis, split_axis=0, concat_axis=0, tiled=True)]
    unnamed x22 -> x20, local copies, waits for them, and re-layouts: 2.7 us -> 7.43 us
    broadcast_in_dim x8 -> x0, local copies, waits for them, and re-layouts: 2.84 us -> none  [copy_for_each(): jnp.broadcast_to(value[None], (length, *value.shape))]
  transfers between devices with their start and end apart: 6 -> 0, of which waited for: 6 -> 0; matrix products, arithmetic and copies ran while one was open for 2% -> 0% of each run, Pallas kernels for 0% -> 0%
where the time goes in v1:
time: 128 us; the launch traced here: 127 us
  Pallas kernels  119 us (93%)
  local copies, waits for them, and re-layouts  7.43 us (6%)
    pallas_call x1, Pallas kernels, per_device(): pl.pallas_call(functools.partial(kernel, n_tp, n_dp), name='decode', out_...  119 us
    unnamed x20, local copies, waits for them, and re-layouts  7.43 us

profile of v1, /device:TPU:33, one launch (start us, length us, event | category | flops | bytes accessed | tf_op | source)
XLA Modules:
  0.0 127.0 jit_solution(11225333505468534948)
XLA Ops:
  0.6 0.0 copy-start
  0.6 0.8 copy.16.decay_offset
  1.4 1.1 copy.13.w_query
  2.5 1.1 copy.14.w_key
  3.6 0.0 copy-start.1
  3.6 0.0 copy-start.4
  3.6 0.0 copy-start.5
  3.6 0.0 copy-start.6
  3.6 1.1 copy.15.w_decay
  4.7 0.0 copy-done
  4.8 0.0 copy-done.1
  4.8 0.0 copy-done.4
  4.8 0.0 copy-done.5
  4.8 0.0 copy-done.6
  4.8 0.0 copy-start.2
  4.8 0.9 copy-done.2
  5.7 0.0 copy-start.3
  5.8 0.9 copy-done.3
  6.7 118.8 %decode.1 = (bf16[3,512]{1,0:T(4,128)(2,1)S(1)}, f32[2,12,1,64,128]{4,3,2,1,0:T(8,128)S(1)}) custom-call(bf16[3,512]{1,0:T(4,128)(2,1)S(1)} %copy-done.4, f32[2,512]{1,0:T(2,128)S(1)} %copy-done.5, bf16[2,512,64]{2,1,0:T(8,128)(2,1)S(1)} %copy.13.w_query, bf16[2,512,64]{2,1,0:T(8,128)(2,1)S(1)} %copy.14.w_key, bf16[2,512,64]{2,1,0:T(8,128)(2,1)S(1)} %copy.15.w_decay, ...), custom_call_target="tpu_custom_call" | custom-call | tf_op jit(solution)/shard_map/decode/pallas_call | solution.py:385
  125.5 0.6 copy.19
  126.1 0.9 copy.20
Async XLA Ops:
  0.6 4.1 %copy-start = (f32[2,12,1,64,128]{4,3,2,1,0:T(8,128)S(1)}, f32[2,12,1,64,128]{4,3,2,1,0:T(8,128)}, u32[]{:S(2)}) copy-start(f32[2,12,1,64,128]{4,3,2,1,0:T(8,128)} %state.1) | copy-start | bytes 2359300
  3.6 1.2 copy-start.1
  3.6 1.2 copy-start.4
  3.6 1.2 copy-start.5
  3.6 1.2 copy-start.6
  4.8 1.0 copy-start.2
  5.7 0.9 copy-start.3

commit v2 on v1

--- a/solution.py
+++ b/solution.py
@@ -36,8 +36,8 @@
     new_state,
     h_v,
     gain_v,
-    qkd_v,
-    wcat,
+    wqkd,
+    wvg,
     ogain_v,
     wout_v,
     off_v,
@@ -93,11 +93,11 @@
     fetches = [
         pltpu.make_async_copy(hidden, h_v, local_sem.at[0]),
         pltpu.make_async_copy(gain, gain_v, local_sem.at[1]),
-        pltpu.make_async_copy(w_query, qkd_v.at[0], local_sem.at[2]),
-        pltpu.make_async_copy(w_key, qkd_v.at[1], local_sem.at[3]),
-        pltpu.make_async_copy(w_decay, qkd_v.at[2], local_sem.at[4]),
-        pltpu.make_async_copy(w_value, wcat.at[:, :, pl.ds(256, 128)], local_sem.at[5]),
-        pltpu.make_async_copy(w_gate, wcat.at[:, :, pl.ds(384, 128)], local_sem.at[6]),
+        pltpu.make_async_copy(w_query, wqkd.at[:, pl.ds(0, HEAD_KEY)], local_sem.at[2]),
+        pltpu.make_async_copy(w_key, wqkd.at[:, pl.ds(HEAD_KEY, HEAD_KEY)], local_sem.at[3]),
+        pltpu.make_async_copy(w_decay, wqkd.at[:, pl.ds(2 * HEAD_KEY, HEAD_KEY)], local_sem.at[4]),
+        pltpu.make_async_copy(w_value, wvg.at[:, :, pl.ds(0, 128)], local_sem.at[5]),
+        pltpu.make_async_copy(w_gate, wvg.at[:, :, pl.ds(128, 128)], local_sem.at[6]),
         pltpu.make_async_copy(out_gain, ogain_v, local_sem.at[7]),
         pltpu.make_async_copy(w_out, wout_v, local_sem.at[8]),
         pltpu.make_async_copy(decay_offset, off_v, local_sem.at[9]),
@@ -109,9 +109,7 @@
     ]
     for f in state_in:
         f.start()
-    for f in fetches:
-        f.wait()
-
+    fetches[0].wait()
     xs[...] = jnp.zeros_like(xs)
 
     first = h_v[...].astype(jnp.float32)
@@ -121,11 +119,7 @@
     pk[0, 1:2, half : half + feats] = first[2:3]
     ag[0, p] = pk[0].astype(jnp.bfloat16)
 
-    for l in range(LAYERS):
-        wcat[l, :, 0:128] = jnp.concatenate([qkd_v[0, l], qkd_v[1, l]], axis=-1)
-        wcat[l, :, 128:256] = jnp.concatenate(
-            [qkd_v[2, l], jnp.zeros_like(qkd_v[2, l])], axis=-1
-        )
+    wqkd[:, 3 * HEAD_KEY :, :] = jnp.zeros_like(wqkd[:, 3 * HEAD_KEY :, :])
 
     pl.semaphore_wait(barrier, n_tp - 1 + n_dp - 1)
 
@@ -191,7 +185,18 @@
         x = xs[...]
         squares = jnp.sum(x * x, axis=1, keepdims=True)[0:seqs]
         scaled = (x * gain_v[l : l + 1, :]).astype(jnp.bfloat16)
-        y = jnp.dot(scaled, wcat[l], preferred_element_type=jnp.float32)[0:seqs]
+        y = jnp.concatenate(
+            [
+                lax.dot_general(
+                    scaled,
+                    wqkd[l],
+                    (((1,), (1,)), ((), ())),
+                    preferred_element_type=jnp.float32,
+                ),
+                jnp.dot(scaled, wvg[l], preferred_element_type=jnp.float32),
+            ],
+            axis=1,
+        )[0:seqs]
         high = squares.astype(jnp.bfloat16).astype(jnp.float32)
         rest = squares - high
         mid = rest.astype(jnp.bfloat16).astype(jnp.float32)
@@ -237,7 +242,7 @@
             value = projected[:, 256:384]
             gate = projected[:, 384:512]
             log_sig = jnp.minimum(decay_pre, 0.0) - jnp.log1p(jnp.exp(-jnp.abs(decay_pre)))
-            rate = jnp.exp(log_sig[:, 0:HEAD_KEY] / softness_factor + off_v[l])
+            rate = jnp.exp(log_sig[:, 0:HEAD_KEY] / softness_factor + off_v[:, l, :])
             columns_qk = jnp.transpose(query_key, (1, 0))
             columns_rate = jnp.transpose(jnp.concatenate([rate, rate], axis=1), (1, 0))
             outs = []
@@ -306,6 +311,9 @@
     lead = n_dp // 2
     for l in range(LAYERS):
         gather_start(l)
+        if l == 0:
+            for f in fetches[1:]:
+                f.wait()
 
         def arrive(i):
             sg = source_group(i)
@@ -378,7 +386,12 @@
     members = n_tp // n_dp
     seqs = state.shape[1]
     block = (2, rows * feats // 2)
-    any_spec = pl.BlockSpec(memory_space=pl.ANY)
+    hbm_spec = pl.BlockSpec(memory_space=pltpu.HBM)
+    vmem_spec = pl.BlockSpec(memory_space=pltpu.VMEM)
+    args = list(args)
+    for i in (2, 3, 4):
+        args[i] = jnp.swapaxes(args[i], 1, 2)
+    args[9] = jnp.swapaxes(args[9], 0, 1)
     bf16, f32 = jnp.bfloat16, jnp.float32
     cols = 512
     dma = pltpu.SemaphoreType.DMA
@@ -389,13 +402,13 @@
             jax.ShapeDtypeStruct(hidden.shape, hidden.dtype),
             jax.ShapeDtypeStruct(state.shape, state.dtype),
         ),
-        in_specs=[any_spec] * 11,
-        out_specs=(pl.BlockSpec(memory_space=pltpu.VMEM), any_spec),
+        in_specs=[hbm_spec] * 11,
+        out_specs=(vmem_spec, hbm_spec),
         scratch_shapes=[
             pltpu.VMEM(hidden.shape, bf16),
             pltpu.VMEM(args[1].shape, f32),
-            pltpu.VMEM((3,) + args[2].shape, bf16),
-            pltpu.VMEM((LAYERS, feats, cols), bf16),
+            pltpu.VMEM((LAYERS, 4 * HEAD_KEY, feats), bf16),
+            pltpu.VMEM((LAYERS, feats, 2 * VALUE_CHANNELS), bf16),
             pltpu.VMEM(args[7].shape, f32),
             pltpu.VMEM(args[8].shape, bf16),
             pltpu.VMEM(args[9].shape, f32),
@@ -421,7 +434,7 @@
             dma((LAYERS,)),
         ],
         compiler_params=pltpu.CompilerParams(
-            collective_id=0, has_side_effects=True, vmem_limit_bytes=32 * 1024 * 1024
+            collective_id=0, has_side_effects=True, vmem_limit_bytes=64000000
         ),
     )(*args)
 

time: 128 us -> 123 us (0.961)
  local copies, waits for them, and re-layouts: 7.43 us -> 3.36 us
    unnamed x20 -> x2, local copies, waits for them, and re-layouts: 7.43 us -> 3.36 us
where the time goes in v2:
time: 123 us
  Pallas kernels  119 us (97%)
  local copies, waits for them, and re-layouts  3.36 us (3%)
    pallas_call x1, Pallas kernels, per_device(): pl.pallas_call(functools.partial(kernel, n_tp, n_dp), name='decode', out_...  119 us
    unnamed x2, local copies, waits for them, and re-layouts  3.36 us

profile of v2, /device:TPU:33, one launch (start us, length us, event | category | flops | bytes accessed | tf_op | source)
XLA Modules:
  0.0 122.9 jit_solution(12852879472181912899)
XLA Ops:
  0.6 118.9 %decode.1 = (bf16[3,512]{1,0:T(4,128)(2,1)}, f32[2,12,1,64,128]{4,3,2,1,0:T(8,128)}) custom-call(bf16[3,512]{1,0:T(4,128)(2,1)} %hidden.1, f32[2,512]{1,0:T(2,128)} %gain.1, bf16[2,64,512]{2,1,0:T(8,128)(2,1)} %bitcast.4, bf16[2,64,512]{2,1,0:T(8,128)(2,1)} %bitcast.5, bf16[2,64,512]{2,1,0:T(8,128)(2,1)} %bitcast.6, bf16[2,512,128]{2,1,0:T(8,128)(2,1)} %w_value.1, ...), custom_call_target="tpu_custom_call" | custom-call | tf_op jit(solution)/shard_map/decode/pallas_call | solution.py:398
  119.5 1.3 %copy.15 = bf16[3,512]{1,0:T(4,128)(2,1)} copy(bf16[3,512]{1,0:T(4,128)(2,1)} %get-tuple-element.4) | data formatting | bytes 6144
  120.8 2.1 %copy.16 = f32[2,12,1,64,128]{4,3,2,1,0:T(8,128)} copy(f32[2,12,1,64,128]{4,3,2,1,0:T(8,128)} %get-tuple-element.5) | data formatting | bytes 1572864

commit v3 on v2

v3 whole, which is shorter than its diff:
```python
import functools

import jax
import jax.numpy as jnp
from jax import lax
from jax.experimental import pallas as pl
from jax.experimental.pallas import tpu as pltpu
from jax.sharding import PartitionSpec as P

D = 4096
HEAD_KEY = 64
VALUE_CHANNELS = 128
LAYERS = 2

epsilon = 1e-06
softness_factor = 16.0

MESH = pl.DeviceIdType.MESH


def kernel(
    n_tp,
    n_dp,
    hidden,
    gain,
    w_query,
    w_key,
    w_decay,
    w_value,
    w_gate,
    out_gain,
    w_out,
    decay_offset,
    state,
    hidden_out,
    new_state,
    h_v,
    gain_v,
    wqkd,
    wvg,
    ogain_v,
    wout_v,
    off_v,
    st,
    ag,
    part_send,
    part_recv,
    gat,
    terms,
    terms_in,
    sums,
    sums_in,
    xs,
    pk,
    local_sem,
    state_sem,
    far_send_sem,
    far_sem,
    mate_send_sem,
    mate_sem,
    part_send_sem,
    part_sem,
    gat_send_sem,
    gat_sem,
    terms_send_sem,
    terms_sem,
    sums_send_sem,
    sums_sem,
):
    rows, feats = h_v.shape
    half = feats // 2
    members = n_tp // n_dp
    seqs = rows * members
    p = lax.axis_index("tp")
    d = lax.axis_index("dp")
    group = p // members
    place = p % members
    anti = (p + n_tp // 2) % n_tp
    last = n_dp - 1

    def mate(j):
        return group * members + (place + 1 + j) % members

    barrier = pltpu.get_barrier_semaphore()
    greeted = [{"tp": mate(j)} for j in range(members - 1)]
    greeted += [{"tp": (p + members) % n_tp}, {"tp": (p - members + n_tp) % n_tp}]
    greeted += [{"dp": (d + 1 + j) % n_dp} for j in range(n_dp - 1)]
    for device in greeted:
        pl.semaphore_signal(barrier, inc=1, device_id=device, device_id_type=MESH)

    fetches = [
        pltpu.make_async_copy(hidden, h_v, local_sem.at[0]),
        pltpu.make_async_copy(gain, gain_v, local_sem.at[1]),
        pltpu.make_async_copy(w_query, wqkd.at[:, pl.ds(0, HEAD_KEY)], local_sem.at[2]),
        pltpu.make_async_copy(w_key, wqkd.at[:, pl.ds(HEAD_KEY, HEAD_KEY)], local_sem.at[3]),
        pltpu.make_async_copy(w_decay, wqkd.at[:, pl.ds(2 * HEAD_KEY, HEAD_KEY)], local_sem.at[4]),
        pltpu.make_async_copy(w_value, wvg.at[:, :, pl.ds(0, 128)], local_sem.at[5]),
        pltpu.make_async_copy(w_gate, wvg.at[:, :, pl.ds(128, 128)], local_sem.at[6]),
        pltpu.make_async_copy(out_gain, ogain_v, local_sem.at[7]),
        pltpu.make_async_copy(w_out, wout_v, local_sem.at[8]),
        pltpu.make_async_copy(decay_offset, off_v, local_sem.at[9]),
    ]
    for f in fetches:
        f.start()
    state_in = [
        pltpu.make_async_copy(state.at[l, :, 0], st.at[l], state_sem.at[l]) for l in range(LAYERS)
    ]
    for f in state_in:
        f.start()

    xs[...] = jnp.zeros_like(xs)
    wqkd[:, 3 * HEAD_KEY :, :] = jnp.zeros_like(wqkd[:, 3 * HEAD_KEY :, :])

    fetches[0].wait()
    first = h_v[...].astype(jnp.float32)
    pk[0, 0:1, 0:feats] = first[0:1]
    pk[0, 0:1, feats : feats + half] = first[1:2, 0:half]
    pk[0, 1:2, 0:half] = first[1:2, half:feats]
    pk[0, 1:2, half : half + feats] = first[2:3]
    ag[0, p] = pk[0].astype(jnp.bfloat16)

    with jax.named_scope("barrier"):
        pl.semaphore_wait(barrier, len(greeted))

    def offset(i):
        k = (i + 1) // 2
        return jnp.where(i % 2 == 1, n_dp - k, k)

    def source_group(i):
        return (group + offset(i)) % n_dp

    def row_group(l, i):
        return (source_group(i) + l * (n_dp // 2)) % n_dp

    def source(i):
        return source_group(i) * members + place

    def remote(src, dst, send_sem, recv_sem, device):
        return pltpu.make_async_remote_copy(
            src_ref=src,
            dst_ref=dst,
            send_sem=send_sem,
            recv_sem=recv_sem,
            device_id=device,
            device_id_type=MESH,
        )

    def arrived(ref, sem):
        remote(ref, ref, far_send_sem.at[0], sem, {"tp": anti}).wait_recv()

    def far_copy(l, sigma, i, to):
        return remote(
            ag.at[l, sigma], ag.at[l, sigma], far_send_sem.at[l], far_sem.at[l, i], {"tp": to}
        )

    def up(k):
        return (p + members * k) % n_tp

    def down(k):
        return (p - members * k + n_tp) % n_tp

    def to_mates(l, i):
        sigma = source(i)
        for j in range(members - 1):
            remote(
                ag.at[l, sigma],
                ag.at[l, sigma],
                mate_send_sem.at[l],
                mate_sem.at[l, i],
                {"tp": mate(j)},
            ).start()

    def begin(l):
        if l == 0:
            far_copy(l, p, 1, up(1)).start()
            far_copy(l, p, 2, down(1)).start()
        else:
            for k in range(n_dp // 2, 0, -1):
                far_copy(l, p, 2 * k - 1, up(k)).start()
                if 2 * k < n_dp:
                    far_copy(l, p, 2 * k, down(k)).start()
        to_mates(l, 0)

    def forward(l, i):
        sigma = source(i)
        arrived(ag.at[l, sigma], far_sem.at[l, i])
        if l == 0:

            @pl.when(i + 2 < n_dp)
            def _():
                far_copy(l, sigma, i + 2, jnp.where(i % 2 == 1, up(1), down(1))).start()

        to_mates(l, i)

    lane = lax.broadcasted_iota(jnp.int32, (seqs, 512), 1)

    def project(l, i):
        sg = source_group(i)
        arrived(ag.at[l, pl.ds(0, members - 1)], mate_sem.at[l, i])
        for j in range(members):
            b = ag[l, sg * members + j].astype(jnp.float32)
            xs[3 * j : 3 * j + 1, :] = b[0:1, 0:feats]
            xs[3 * j + 1 : 3 * j + 2, 0:half] = b[0:1, feats : feats + half]
            xs[3 * j + 1 : 3 * j + 2, half:feats] = b[1:2, 0:half]
            xs[3 * j + 2 : 3 * j + 3, :] = b[1:2, half : half + feats]
        x = xs[...]
        squares = jnp.sum(x * x, axis=1, keepdims=True)[0:seqs]
        scaled = (x * gain_v[l : l + 1, :]).astype(jnp.bfloat16)
        y = jnp.concatenate(
            [
                lax.dot_general(
                    scaled,
                    wqkd[l],
                    (((1,), (1,)), ((), ())),
                    preferred_element_type=jnp.float32,
                ),
                jnp.dot(scaled, wvg[l], preferred_element_type=jnp.float32),
            ],
            axis=1,
        )[0:seqs]
        high = squares.astype(jnp.bfloat16).astype(jnp.float32)
        rest = squares - high
        mid = rest.astype(jnp.bfloat16).astype(jnp.float32)
        low = rest - mid
        y = jnp.where(lane == 192, high, y)
        y = jnp.where(lane == 193, mid, y)
        y = jnp.where(lane == 194, low, y)
        part_send[l, i] = y.astype(jnp.bfloat16)
        to = row_group(l, i)

        @pl.when(to != d)
        def _():
            slot = (d - to + n_dp) % n_dp - 1
            remote(
                part_send.at[l, i],
                part_recv.at[l, slot],
                part_send_sem.at[l],
                part_sem.at[l],
                {"dp": to},
            ).start()

    def gat_copy(l, i, peer):
        return remote(
            gat.at[l, i], gat.at[l, i], gat_send_sem.at[l], gat_sem.at[l, i], {"dp": peer}
        )

    def update(l, i):
        arrived(part_recv.at[l], part_sem.at[l])
        total = part_send[l, i].astype(jnp.float32)
        for k in range(n_dp - 1):
            total += part_recv[l, k].astype(jnp.float32)
        squares = jnp.sum(total[:, 192:195], axis=1, keepdims=True)
        projected = total * lax.rsqrt(squares / D + epsilon)
        query_key = projected[:, 0:128]
        decay_pre = projected[:, 128:256]
        value = projected[:, 256:384]
        gate = projected[:, 384:512]
        log_sig = jnp.minimum(decay_pre, 0.0) - jnp.log1p(jnp.exp(-jnp.abs(decay_pre)))
        rate = jnp.exp(log_sig[:, 0:HEAD_KEY] / softness_factor + off_v[:, l, :])
        columns_qk = jnp.transpose(query_key, (1, 0))
        columns_rate = jnp.transpose(jnp.concatenate([rate, rate], axis=1), (1, 0))
        outs = []
        for s in range(seqs):
            q = columns_qk[0:HEAD_KEY, s : s + 1]
            k = columns_qk[HEAD_KEY : 2 * HEAD_KEY, s : s + 1] * HEAD_KEY ** (-0.5)
            r = columns_rate[0:HEAD_KEY, s : s + 1]
            fresh = r * st[l, s] + k * value[s : s + 1, :]
            new_state[l, s, 0] = fresh
            outs.append(jnp.sum(q * fresh, axis=0, keepdims=True))
        readout = jnp.concatenate(outs, axis=0)
        normed = readout * lax.rsqrt(jnp.mean(readout * readout, axis=1, keepdims=True) + epsilon)
        normed = normed * ogain_v[l : l + 1, :]
        silu = gate / (1.0 + jnp.exp(-gate))
        gat[l, i] = (normed * silu).astype(jnp.bfloat16)
        for j in range(n_dp - 1):
            gat_copy(l, i, (d + 1 + j) % n_dp).start()

    def out_project(l, i):
        @pl.when(row_group(l, i) != d)
        def _():
            arrived(gat.at[l, i], gat_sem.at[l, i])

        y = jnp.dot(gat[l, i], wout_v[l], preferred_element_type=jnp.float32)
        for j in range(members):
            pk[j, 0:1, 0:feats] = y[3 * j : 3 * j + 1]
            pk[j, 0:1, feats : feats + half] = y[3 * j + 1 : 3 * j + 2, 0:half]
            pk[j, 1:2, 0:half] = y[3 * j + 1 : 3 * j + 2, half:feats]
            pk[j, 1:2, half : half + feats] = y[3 * j + 2 : 3 * j + 3]
        for j in range(members):
            terms[l, members * i + j] = pk[j].astype(jnp.bfloat16)
        for j in range(members - 1):
            to = (place + 1 + j) % members
            remote(
                terms.at[l, members * i + to],
                terms_in.at[l, (members - 1) * i + members - 2 - j],
                terms_send_sem.at[l],
                terms_sem.at[l, i],
                {"tp": mate(j)},
            ).start()

    def add_quad(l, i):
        arrived(terms_in.at[l, pl.ds(0, members - 1)], terms_sem.at[l, i])
        total = terms[l, members * i + place].astype(jnp.float32)
        for j in range(members - 1):
            total += terms_in[l, (members - 1) * i + j].astype(jnp.float32)
        sums[l, i] = total.astype(jnp.bfloat16)

        @pl.when(i < last)
        def _():
            remote(
                sums.at[l, i],
                sums_in.at[l, i],
                sums_send_sem.at[l],
                sums_sem.at[l],
                {"tp": (source(i) + n_tp // 2) % n_tp},
            ).start()

    def both(fn, l, k):
        for i in (2 * k - 1, 2 * k):

            @pl.when((i >= 0) & (i < n_dp))
            def _():
                fn(l, i)

    def mine(l, k):
        low, high = 2 * k - 1, 2 * k
        at_low = (low >= 0) & (low < n_dp) & (row_group(l, jnp.maximum(low, 0)) == d)
        at_high = (high >= 0) & (high < n_dp) & (row_group(l, jnp.maximum(high, 0)) == d)

        @pl.when(at_low | at_high)
        def _():
            update(l, jnp.where(at_low, low, high))

    def far(l, k):
        @pl.when(k > 0)
        def _():
            both(forward, l, k)

    steps = n_dp // 2
    for l in range(LAYERS):
        begin(l)
        if l == 0:
            for f in fetches[1:]:
                f.wait()
        state_in[l].wait()

        def tick(t, c):
            if l == 0:
                both(project, l, t - 1)
                mine(l, t - 2)
                far(l, t)
                both(out_project, l, t - 3)
                both(add_quad, l, t - 4)
            else:
                far(l, t)
                both(project, l, t - 1)
                both(add_quad, l, t - 5)
                both(out_project, l, t - 4)
                mine(l, t - 2)
            return c

        lax.fori_loop(1, steps + (5 if l == 0 else 6), tick, 0)

        with jax.named_scope("owner_wait"):
            arrived(sums_in.at[l], sums_sem.at[l])
        total = sums[l, last].astype(jnp.float32)
        total += jnp.sum(sums_in[l].astype(jnp.float32), axis=0)
        result = (total + ag[l, anti].astype(jnp.float32)).astype(jnp.bfloat16)
        if l + 1 < LAYERS:
            ag[l + 1, p] = result
        else:
            b = result.astype(jnp.float32)
            xs[0:1, :] = b[0:1, 0:feats]
            xs[1:2, 0:half] = b[0:1, feats : feats + half]
            xs[1:2, half:feats] = b[1:2, 0:half]
            xs[2:3, :] = b[1:2, half : half + feats]
            hidden_out[...] = xs[0:rows, :].astype(jnp.bfloat16)

    for l in range(LAYERS):
        many = (members - 1) * n_dp
        for ref, sem in (
            (sums_in.at[l], far_send_sem),
            (sums_in.at[l], sums_send_sem),
            (ag.at[l, pl.ds(0, many)], mate_send_sem),
            (ag.at[l, pl.ds(0, many)], terms_send_sem),
            (part_recv.at[l], part_send_sem),
            (gat.at[l, pl.ds(0, n_dp - 1)], gat_send_sem),
        ):
            remote(ref, ref, sem.at[l], part_sem.at[l], {"tp": anti}).wait_send()


def store_results(h, s, h_out, s_out, sem):
    copies = [
        pltpu.make_async_copy(s, s_out, sem.at[0]),
        pltpu.make_async_copy(h, h_out, sem.at[1]),
    ]
    for c in copies:
        c.start()
    for c in copies:
        c.wait()


def per_device(n_tp, n_dp, *args):
    hidden, state = args[0], args[10]
    rows, feats = hidden.shape
    members = n_tp // n_dp
    seqs = state.shape[1]
    block = (2, rows * feats // 2)
    hbm_spec = pl.BlockSpec(memory_space=pltpu.HBM)
    vmem_spec = pl.BlockSpec(memory_space=pltpu.VMEM)
    args = list(args)
    for i in (2, 3, 4):
        args[i] = jnp.swapaxes(args[i], 1, 2)
    args[9] = jnp.swapaxes(args[9], 0, 1)
    bf16, f32 = jnp.bfloat16, jnp.float32
    cols = 512
    dma = pltpu.SemaphoreType.DMA
    results = pl.pallas_call(
        functools.partial(kernel, n_tp, n_dp),
        name="decode",
        out_shape=(
            pltpu.VMEM(hidden.shape, hidden.dtype),
            pltpu.VMEM(state.shape, state.dtype),
        ),
        in_specs=[hbm_spec] * 11,
        out_specs=(vmem_spec, vmem_spec),
        scratch_shapes=[
            pltpu.VMEM(hidden.shape, bf16),
            pltpu.VMEM(args[1].shape, f32),
            pltpu.VMEM((LAYERS, 4 * HEAD_KEY, feats), bf16),
            pltpu.VMEM((LAYERS, feats, 2 * VALUE_CHANNELS), bf16),
            pltpu.VMEM(args[7].shape, f32),
            pltpu.VMEM(args[8].shape, bf16),
            pltpu.VMEM(args[9].shape, f32),
            pltpu.VMEM((LAYERS, seqs) + state.shape[3:], f32),
            pltpu.VMEM((LAYERS, n_tp) + block, bf16),
            pltpu.VMEM((LAYERS, n_dp, seqs, cols), bf16),
            pltpu.VMEM((LAYERS, n_dp - 1, seqs, cols), bf16),
            pltpu.VMEM((LAYERS, n_dp, seqs, VALUE_CHANNELS), bf16),
            pltpu.VMEM((LAYERS, n_tp) + block, bf16),
            pltpu.VMEM((LAYERS, n_dp * (members - 1)) + block, bf16),
            pltpu.VMEM((LAYERS, n_dp) + block, bf16),
            pltpu.VMEM((LAYERS, n_dp - 1) + block, bf16),
            pltpu.VMEM((16, feats), f32),
            pltpu.VMEM((members,) + block, f32),
            dma((10,)),
            dma((LAYERS,)),
            dma((LAYERS,)),
            dma((LAYERS, n_dp)),
            dma((LAYERS,)),
            dma((LAYERS, n_dp)),
            dma((LAYERS,)),
            dma((LAYERS,)),
            dma((LAYERS,)),
            dma((LAYERS, n_dp)),
            dma((LAYERS,)),
            dma((LAYERS, n_dp)),
            dma((LAYERS,)),
            dma((LAYERS,)),
        ],
        compiler_params=pltpu.CompilerParams(
            collective_id=0, has_side_effects=True, vmem_limit_bytes=64000000
        ),
    )(*args)
    return pl.pallas_call(
        store_results,
        name="store_results",
        out_shape=tuple(jax.ShapeDtypeStruct(r.shape, r.dtype) for r in (hidden, state)),
        in_specs=[vmem_spec] * 2,
        out_specs=(hbm_spec, hbm_spec),
        scratch_shapes=[dma((2,))],
    )(*[pltpu.with_memory_space_constraint(r, pltpu.VMEM) for r in results])


def solution(mesh):
    return jax.shard_map(
        functools.partial(per_device, mesh.shape["tp"], mesh.shape["dp"]),
        mesh=mesh,
        in_specs=(
            P(("grp", "tp"), "dp"),
            P(None, "dp"),
            P(None, "dp", "tp"),
            P(None, "dp", "tp"),
            P(None, "dp", "tp"),
            P(None, "dp", "tp"),
            P(None, "dp", "tp"),
            P(None, "tp"),
            P(None, "tp", "dp"),
            P(None, ("grp", "dp"), "tp"),
            P(None, ("grp", "dp"), "tp", None, None),
        ),
        out_specs=(P(("grp", "tp"), "dp"), P(None, ("grp", "dp"), "tp", None, None)),
        check_vma=False,
    )
```

time: 123 us -> 117 us (0.951); the launches traced: 123 us -> 115 us
  Pallas kernels: 119 us -> 114 us
  local copies, waits for them, and re-layouts: 3.36 us -> 0 us
    pallas_call x1, Pallas kernels: 119 us -> 113 us  [per_device(): pl.pallas_call(functools.partial(kernel, n_tp, n_dp), name='decode', out_...]
    unnamed x2 -> x0, local copies, waits for them, and re-layouts: 3.36 us -> none
where the time goes in v3:
time: 117 us; the launch traced here: 115 us
  Pallas kernels  114 us (97%)
    pallas_call x1, Pallas kernels, per_device(): pl.pallas_call(functools.partial(kernel, n_tp, n_dp), name='decode', out_...  113 us

profile of v3, /device:TPU:33, one launch (start us, length us, event | category | flops | bytes accessed | tf_op | source)
XLA Modules:
  0.0 114.9 jit_solution(7888341263262053722)
XLA Ops:
  0.6 113.3 %decode.1 = (bf16[3,512]{1,0:T(4,128)(2,1)S(1)}, f32[2,12,1,64,128]{4,3,2,1,0:T(8,128)S(1)}) custom-call(bf16[3,512]{1,0:T(4,128)(2,1)} %hidden.1, f32[2,512]{1,0:T(2,128)} %gain.1, bf16[2,64,512]{2,1,0:T(8,128)(2,1)} %bitcast.4, bf16[2,64,512]{2,1,0:T(8,128)(2,1)} %bitcast.5, bf16[2,64,512]{2,1,0:T(8,128)(2,1)} %bitcast.6, bf16[2,512,128]{2,1,0:T(8,128)(2,1)} %w_value.1, ...), custom_call_target="tpu_custom_call" | custom-call | tf_op jit(solution)/shard_map/decode/pallas_call | solution.py:418
  114.0 0.9 store_results.1

commit v4 on v3

--- a/solution.py
+++ b/solution.py
@@ -16,6 +16,19 @@
 softness_factor = 16.0
 
 MESH = pl.DeviceIdType.MESH
+
+STEPS = (
+    (
+        "A0", "F1", "F2", "A1", "F3", "A2", "U0", "A3",
+        "F4", "U1", "O0", "U3", "U2", "A4", "O1", "O2",
+        "U4", "O3", "O4",
+    ),
+    (
+        "F1", "A0", "F2", "A1", "U0", "F3", "A2", "U1",
+        "F4", "A3", "O0", "U2", "O1", "A4", "U3", "O2",
+        "U4", "O3", "O4",
+    ),
+)
 
 
 def kernel(
@@ -48,8 +61,6 @@
     gat,
     terms,
     terms_in,
-    sums,
-    sums_in,
     xs,
     pk,
     local_sem,
@@ -64,8 +75,6 @@
     gat_sem,
     terms_send_sem,
     terms_sem,
-    sums_send_sem,
-    sums_sem,
 ):
     rows, feats = h_v.shape
     half = feats // 2
@@ -184,11 +193,8 @@
     def forward(l, i):
         sigma = source(i)
         arrived(ag.at[l, sigma], far_sem.at[l, i])
-        if l == 0:
-
-            @pl.when(i + 2 < n_dp)
-            def _():
-                far_copy(l, sigma, i + 2, jnp.where(i % 2 == 1, up(1), down(1))).start()
+        if l == 0 and i + 2 < n_dp:
+            far_copy(l, sigma, i + 2, up(1) if i % 2 == 1 else down(1)).start()
 
         to_mates(l, i)
 
@@ -288,83 +294,49 @@
             pk[j, 1:2, half : half + feats] = y[3 * j + 2 : 3 * j + 3]
         for j in range(members):
             terms[l, members * i + j] = pk[j].astype(jnp.bfloat16)
-        for j in range(members - 1):
-            to = (place + 1 + j) % members
-            remote(
-                terms.at[l, members * i + to],
-                terms_in.at[l, (members - 1) * i + members - 2 - j],
-                terms_send_sem.at[l],
-                terms_sem.at[l, i],
-                {"tp": mate(j)},
-            ).start()
-
-    def add_quad(l, i):
-        arrived(terms_in.at[l, pl.ds(0, members - 1)], terms_sem.at[l, i])
-        total = terms[l, members * i + place].astype(jnp.float32)
-        for j in range(members - 1):
-            total += terms_in[l, (members - 1) * i + j].astype(jnp.float32)
-        sums[l, i] = total.astype(jnp.bfloat16)
-
-        @pl.when(i < last)
+        base = source_group(i) * members + n_tp // 2
+        for j in range(members):
+            owner = (base + j) % n_tp
+
+            @pl.when(owner != p)
+            def _():
+                remote(
+                    terms.at[l, members * i + j],
+                    terms_in.at[l, (p - owner + n_tp) % n_tp - 1],
+                    terms_send_sem.at[l],
+                    terms_sem.at[l],
+                    {"tp": owner},
+                ).start()
+
+    def nearby(k):
+        return [i for i in (2 * k - 1, 2 * k) if 0 <= i < n_dp]
+
+    def mine(l, k):
+        wanted = [row_group(l, i) == d for i in nearby(k)]
+
+        @pl.when(functools.reduce(jnp.logical_or, wanted))
         def _():
-            remote(
-                sums.at[l, i],
-                sums_in.at[l, i],
-                sums_send_sem.at[l],
-                sums_sem.at[l],
-                {"tp": (source(i) + n_tp // 2) % n_tp},
-            ).start()
-
-    def both(fn, l, k):
-        for i in (2 * k - 1, 2 * k):
-
-            @pl.when((i >= 0) & (i < n_dp))
-            def _():
-                fn(l, i)
-
-    def mine(l, k):
-        low, high = 2 * k - 1, 2 * k
-        at_low = (low >= 0) & (low < n_dp) & (row_group(l, jnp.maximum(low, 0)) == d)
-        at_high = (high >= 0) & (high < n_dp) & (row_group(l, jnp.maximum(high, 0)) == d)
-
-        @pl.when(at_low | at_high)
-        def _():
-            update(l, jnp.where(at_low, low, high))
-
-    def far(l, k):
-        @pl.when(k > 0)
-        def _():
-            both(forward, l, k)
-
-    steps = n_dp // 2
+            update(l, jnp.where(wanted[0], nearby(k)[0], nearby(k)[-1]))
+
     for l in range(LAYERS):
         begin(l)
         if l == 0:
             for f in fetches[1:]:
                 f.wait()
         state_in[l].wait()
-
-        def tick(t, c):
-            if l == 0:
-                both(project, l, t - 1)
-                mine(l, t - 2)
-                far(l, t)
-                both(out_project, l, t - 3)
-                both(add_quad, l, t - 4)
+        for step in STEPS[l]:
+            k = int(step[1:])
+            if step[0] == "U":
+                mine(l, k)
             else:
-                far(l, t)
-                both(project, l, t - 1)
-                both(add_quad, l, t - 5)
-                both(out_project, l, t - 4)
-                mine(l, t - 2)
-            return c
-
-        lax.fori_loop(1, steps + (5 if l == 0 else 6), tick, 0)
+                fn = {"F": forward, "A": project, "O": out_project}[step[0]]
+                for i in nearby(k):
+                    fn(l, i)
 
         with jax.named_scope("owner_wait"):
-            arrived(sums_in.at[l], sums_sem.at[l])
-        total = sums[l, last].astype(jnp.float32)
-        total += jnp.sum(sums_in[l].astype(jnp.float32), axis=0)
+            arrived(terms_in.at[l], terms_sem.at[l])
+        total = terms[l, members * last + place].astype(jnp.float32)
+        total += jnp.sum(terms_in[l].astype(jnp.float32), axis=0)
         result = (total + ag[l, anti].astype(jnp.float32)).astype(jnp.bfloat16)
         if l + 1 < LAYERS:
             ag[l + 1, p] = result
@@ -379,10 +351,9 @@
     for l in range(LAYERS):
         many = (members - 1) * n_dp
         for ref, sem in (
-            (sums_in.at[l], far_send_sem),
-            (sums_in.at[l], sums_send_sem),
+            (ag.at[l, pl.ds(0, n_dp - 1)], far_send_sem),
             (ag.at[l, pl.ds(0, many)], mate_send_sem),
-            (ag.at[l, pl.ds(0, many)], terms_send_sem),
+            (terms_in.at[l], terms_send_sem),
             (part_recv.at[l], part_send_sem),
             (gat.at[l, pl.ds(0, n_dp - 1)], gat_send_sem),
         ):
@@ -438,9 +409,7 @@
             pltpu.VMEM((LAYERS, n_dp - 1, seqs, cols), bf16),
             pltpu.VMEM((LAYERS, n_dp, seqs, VALUE_CHANNELS), bf16),
             pltpu.VMEM((LAYERS, n_tp) + block, bf16),
-            pltpu.VMEM((LAYERS, n_dp * (members - 1)) + block, bf16),
-            pltpu.VMEM((LAYERS, n_dp) + block, bf16),
-            pltpu.VMEM((LAYERS, n_dp - 1) + block, bf16),
+            pltpu.VMEM((LAYERS, n_tp - 1) + block, bf16),
             pltpu.VMEM((16, feats), f32),
             pltpu.VMEM((members,) + block, f32),
             dma((10,)),
@@ -451,8 +420,6 @@
             dma((LAYERS, n_dp)),
             dma((LAYERS,)),
             dma((LAYERS,)),
-            dma((LAYERS,)),
-            dma((LAYERS, n_dp)),
             dma((LAYERS,)),
             dma((LAYERS, n_dp)),
             dma((LAYERS,)),

time: 117 us -> 115 us (0.983); the launches traced: 115 us -> 115 us
  no operation moved by 1% of the time
where the time goes in v4:
time: 115 us
  Pallas kernels  114 us (99%)
    pallas_call x1, Pallas kernels, per_device(): pl.pallas_call(functools.partial(kernel, n_tp, n_dp), name='decode', out_...  113 us

profile of v4, /device:TPU:33, one launch (start us, length us, event | category | flops | bytes accessed | tf_op | source)
XLA Modules:
  0.0 114.8 jit_solution(5814274635438630531)
XLA Ops:
  0.6 113.3 %decode.1 = (bf16[3,512]{1,0:T(4,128)(2,1)S(1)}, f32[2,12,1,64,128]{4,3,2,1,0:T(8,128)S(1)}) custom-call(bf16[3,512]{1,0:T(4,128)(2,1)} %hidden.1, f32[2,512]{1,0:T(2,128)} %gain.1, bf16[2,64,512]{2,1,0:T(8,128)(2,1)} %bitcast.4, bf16[2,64,512]{2,1,0:T(8,128)(2,1)} %bitcast.5, bf16[2,64,512]{2,1,0:T(8,128)(2,1)} %bitcast.6, bf16[2,512,128]{2,1,0:T(8,128)(2,1)} %w_value.1, ...), custom_call_target="tpu_custom_call" | custom-call | tf_op jit(solution)/shard_map/decode/pallas_call | solution.py:389
  113.9 0.9 store_results.1

commit v5 on v4

--- a/solution.py
+++ b/solution.py
@@ -19,12 +19,12 @@
 
 STEPS = (
     (
-        "A0", "F1", "F2", "A1", "F3", "A2", "U0", "A3",
-        "F4", "U1", "O0", "U3", "U2", "A4", "O1", "O2",
+        "A0", "F1", "F2", "A1", "U0", "F3", "A2", "U1",
+        "F4", "O0", "A3", "U2", "O1", "A4", "U3", "O2",
         "U4", "O3", "O4",
     ),
     (
-        "F1", "A0", "F2", "A1", "U0", "F3", "A2", "U1",
+        "A0", "F1", "F2", "U0", "A1", "F3", "A2", "U1",
         "F4", "A3", "O0", "U2", "O1", "A4", "U3", "O2",
         "U4", "O3", "O4",
     ),
@@ -65,6 +65,8 @@
     pk,
     local_sem,
     state_sem,
+    ready,
+    all_send_sem,
     far_send_sem,
     far_sem,
     mate_send_sem,
@@ -90,12 +92,31 @@
     def mate(j):
         return group * members + (place + 1 + j) % members
 
+    def up(k):
+        return (p + members * k) % n_tp
+
+    def down(k):
+        return (p - members * k + n_tp) % n_tp
+
+    quads = [up(k) for k in range(1, n_dp // 2 + 1)] + [down(k) for k in range(1, n_dp // 2)]
     barrier = pltpu.get_barrier_semaphore()
-    greeted = [{"tp": mate(j)} for j in range(members - 1)]
-    greeted += [{"tp": (p + members) % n_tp}, {"tp": (p - members + n_tp) % n_tp}]
-    greeted += [{"dp": (d + 1 + j) % n_dp} for j in range(n_dp - 1)]
-    for device in greeted:
+
+    def greet(device):
         pl.semaphore_signal(barrier, inc=1, device_id=device, device_id_type=MESH)
+
+    for j in range(members - 1):
+        greet({"tp": mate(j)})
+    for peer in quads:
+
+        @pl.when((peer > p) | (peer == p - members))
+        def _():
+            greet({"tp": peer})
+
+    for j in range(n_dp - 1):
+        greet({"dp": (d + 1 + j) % n_dp})
+    heard = members - 1 + n_dp - 1
+    for peer in quads:
+        heard += jnp.where((peer < p) | (peer == p + members), 1, 0)
 
     fetches = [
         pltpu.make_async_copy(hidden, h_v, local_sem.at[0]),
@@ -129,7 +150,11 @@
     ag[0, p] = pk[0].astype(jnp.bfloat16)
 
     with jax.named_scope("barrier"):
-        pl.semaphore_wait(barrier, len(greeted))
+        pl.semaphore_wait(barrier, heard)
+
+    @pl.when(up(1) < p)
+    def _():
+        pl.semaphore_signal(ready, inc=1, device_id={"tp": up(1)}, device_id_type=MESH)
 
     def offset(i):
         k = (i + 1) // 2
@@ -155,18 +180,35 @@
         )
 
     def arrived(ref, sem):
-        remote(ref, ref, far_send_sem.at[0], sem, {"tp": anti}).wait_recv()
-
-    def far_copy(l, sigma, i, to):
+        remote(ref, ref, all_send_sem, sem, {"tp": anti}).wait_recv()
+
+    def far_copy(sigma, i, to, relayed):
         return remote(
-            ag.at[l, sigma], ag.at[l, sigma], far_send_sem.at[l], far_sem.at[l, i], {"tp": to}
+            ag.at[0, sigma], ag.at[0, sigma], far_send_sem.at[relayed, i], far_sem.at[0, i], {"tp": to}
         )
 
-    def up(k):
-        return (p + members * k) % n_tp
-
-    def down(k):
-        return (p - members * k + n_tp) % n_tp
+    def own_rows(act):
+        for k in range(n_dp // 2, 0, -1):
+            for i, to in ((2 * k - 1, up(k)), (2 * k, down(k))):
+                if i == n_dp:
+                    continue
+
+                @pl.when((to < p) | (to == p + members))
+                def _():
+                    act(far_copy(p, i, to, 0))
+
+    def across(act):
+        @pl.when(down(1) > p)
+        def _():
+            act(far_copy(p, 2, down(1), 0))
+
+    def relay(i, act):
+        sigma = source(i)
+        to = up(1) if i % 2 == 1 else down(1)
+
+        @pl.when(to > sigma)
+        def _():
+            act(far_copy(sigma, i + 2, to, 1))
 
     def to_mates(l, i):
         sigma = source(i)
@@ -181,21 +223,27 @@
 
     def begin(l):
         if l == 0:
-            far_copy(l, p, 1, up(1)).start()
-            far_copy(l, p, 2, down(1)).start()
+            own_rows(lambda copy: copy.start())
+            to_mates(l, 0)
+
+            @pl.when(down(1) > p)
+            def _():
+                pl.semaphore_wait(ready, 1)
+
+            across(lambda copy: copy.start())
         else:
             for k in range(n_dp // 2, 0, -1):
-                far_copy(l, p, 2 * k - 1, up(k)).start()
-                if 2 * k < n_dp:
-                    far_copy(l, p, 2 * k, down(k)).start()
-        to_mates(l, 0)
+                for i, to in ((2 * k - 1, up(k)), (2 * k, down(k))):
+                    if i < n_dp:
+                        remote(
+                            ag.at[l, p], ag.at[l, p], all_send_sem, far_sem.at[l, i], {"tp": to}
+                        ).start()
+            to_mates(l, 0)
 
     def forward(l, i):
-        sigma = source(i)
-        arrived(ag.at[l, sigma], far_sem.at[l, i])
+        arrived(ag.at[l, source(i)], far_sem.at[l, i])
         if l == 0 and i + 2 < n_dp:
-            far_copy(l, sigma, i + 2, up(1) if i % 2 == 1 else down(1)).start()
-
+            relay(i, lambda copy: copy.start())
         to_mates(l, i)
 
     lane = lax.broadcasted_iota(jnp.int32, (seqs, 512), 1)
@@ -263,23 +311,26 @@
         gate = projected[:, 384:512]
         log_sig = jnp.minimum(decay_pre, 0.0) - jnp.log1p(jnp.exp(-jnp.abs(decay_pre)))
         rate = jnp.exp(log_sig[:, 0:HEAD_KEY] / softness_factor + off_v[:, l, :])
-        columns_qk = jnp.transpose(query_key, (1, 0))
-        columns_rate = jnp.transpose(jnp.concatenate([rate, rate], axis=1), (1, 0))
+        query = query_key[:, 0:HEAD_KEY]
+        key = query_key[:, HEAD_KEY : 2 * HEAD_KEY] * HEAD_KEY ** (-0.5)
+        columns = jnp.transpose(jnp.concatenate([query * rate, rate], axis=1), (1, 0))
         outs = []
         for s in range(seqs):
-            q = columns_qk[0:HEAD_KEY, s : s + 1]
-            k = columns_qk[HEAD_KEY : 2 * HEAD_KEY, s : s + 1] * HEAD_KEY ** (-0.5)
-            r = columns_rate[0:HEAD_KEY, s : s + 1]
-            fresh = r * st[l, s] + k * value[s : s + 1, :]
-            new_state[l, s, 0] = fresh
-            outs.append(jnp.sum(q * fresh, axis=0, keepdims=True))
+            weight = columns[0:HEAD_KEY, s : s + 1]
+            outs.append(jnp.sum(weight * st[l, s], axis=0, keepdims=True))
         readout = jnp.concatenate(outs, axis=0)
+        readout += jnp.sum(query * key, axis=1, keepdims=True) * value
         normed = readout * lax.rsqrt(jnp.mean(readout * readout, axis=1, keepdims=True) + epsilon)
         normed = normed * ogain_v[l : l + 1, :]
         silu = gate / (1.0 + jnp.exp(-gate))
         gat[l, i] = (normed * silu).astype(jnp.bfloat16)
         for j in range(n_dp - 1):
             gat_copy(l, i, (d + 1 + j) % n_dp).start()
+        columns_key = jnp.transpose(jnp.concatenate([key, key], axis=1), (1, 0))
+        for s in range(seqs):
+            r = columns[HEAD_KEY : 2 * HEAD_KEY, s : s + 1]
+            k = columns_key[0:HEAD_KEY, s : s + 1]
+            new_state[l, s, 0] = r * st[l, s] + k * value[s : s + 1, :]
 
     def out_project(l, i):
         @pl.when(row_group(l, i) != d)
@@ -349,15 +400,22 @@
             hidden_out[...] = xs[0:rows, :].astype(jnp.bfloat16)
 
     for l in range(LAYERS):
-        many = (members - 1) * n_dp
         for ref, sem in (
-            (ag.at[l, pl.ds(0, n_dp - 1)], far_send_sem),
-            (ag.at[l, pl.ds(0, many)], mate_send_sem),
             (terms_in.at[l], terms_send_sem),
             (part_recv.at[l], part_send_sem),
             (gat.at[l, pl.ds(0, n_dp - 1)], gat_send_sem),
         ):
             remote(ref, ref, sem.at[l], part_sem.at[l], {"tp": anti}).wait_send()
+    for ref, sem in (
+        (ag.at[0, pl.ds(0, (members - 1) * n_dp)], mate_send_sem.at[0]),
+        (ag.at[1, pl.ds(0, (members - 1) * n_dp)], mate_send_sem.at[1]),
+        (ag.at[1, pl.ds(0, n_dp - 1)], all_send_sem),
+    ):
+        remote(ref, ref, sem, part_sem.at[0], {"tp": anti}).wait_send()
+    own_rows(lambda copy: copy.wait_send())
+    across(lambda copy: copy.wait_send())
+    for i in range(1, n_dp - 2):
+        relay(i, lambda copy: copy.wait_send())
 
 
 def store_results(h, s, h_out, s_out, sem):
@@ -414,7 +472,9 @@
             pltpu.VMEM((members,) + block, f32),
             dma((10,)),
             dma((LAYERS,)),
-            dma((LAYERS,)),
+            pltpu.SemaphoreType.REGULAR,
+            dma(()),
+            dma((2, n_dp)),
             dma((LAYERS, n_dp)),
             dma((LAYERS,)),
             dma((LAYERS, n_dp)),

time: 115 us -> 115 us (level)
  no operation moved by 1% of the time
where the time goes in v5:
time: 115 us
  Pallas kernels  114 us (99%)
    pallas_call x1, Pallas kernels, per_device(): pl.pallas_call(functools.partial(kernel, n_tp, n_dp), name='decode', out_...  113 us

profile of v5, /device:TPU:33, one launch (start us, length us, event | category | flops | bytes accessed | tf_op | source)
XLA Modules:
  0.0 114.9 jit_solution(11278274692005451142)
XLA Ops:
  0.6 113.4 %decode.1 = (bf16[3,512]{1,0:T(4,128)(2,1)S(1)}, f32[2,12,1,64,128]{4,3,2,1,0:T(8,128)S(1)}) custom-call(bf16[3,512]{1,0:T(4,128)(2,1)} %hidden.1, f32[2,512]{1,0:T(2,128)} %gain.1, bf16[2,64,512]{2,1,0:T(8,128)(2,1)} %bitcast.4, bf16[2,64,512]{2,1,0:T(8,128)(2,1)} %bitcast.5, bf16[2,64,512]{2,1,0:T(8,128)(2,1)} %bitcast.6, bf16[2,512,128]{2,1,0:T(8,128)(2,1)} %w_value.1, ...), custom_call_target="tpu_custom_call" | custom-call | tf_op jit(solution)/shard_map/decode/pallas_call | solution.py:447
  114.0 0.9 store_results.1

commit v6 on v5

--- a/solution.py
+++ b/solution.py
@@ -19,14 +19,14 @@
 
 STEPS = (
     (
-        "A0", "F1", "F2", "A1", "U0", "F3", "A2", "U1",
-        "F4", "O0", "A3", "U2", "O1", "A4", "U3", "O2",
+        "F1", "A0", "F2", "A1", "F3", "U0", "A2", "F4",
+        "U1", "A3", "O0", "U2", "O1", "A4", "U3", "O2",
         "U4", "O3", "O4",
     ),
     (
-        "A0", "F1", "F2", "U0", "A1", "F3", "A2", "U1",
-        "F4", "A3", "O0", "U2", "O1", "A4", "U3", "O2",
-        "U4", "O3", "O4",
+        "F1", "A0", "F2", "A1", "F3", "U0", "A2", "F4",
+        "U1", "A3", "O0", "U2", "A4", "O1", "U3", "U4",
+        "O2", "O3", "O4",
     ),
 )
 

time: 115 us -> 115 us (level)
  no operation moved by 1% of the time
where the time goes in v6:
time: 115 us
  Pallas kernels  114 us (99%)
    pallas_call x1, Pallas kernels, per_device(): pl.pallas_call(functools.partial(kernel, n_tp, n_dp), name='decode', out_...  113 us

profile of v6, /device:TPU:33, one launch (start us, length us, event | category | flops | bytes accessed | tf_op | source)
XLA Modules:
  0.0 114.6 jit_solution(18114448474923676088)
XLA Ops:
  0.6 113.0 %decode.1 = (bf16[3,512]{1,0:T(4,128)(2,1)S(1)}, f32[2,12,1,64,128]{4,3,2,1,0:T(8,128)S(1)}) custom-call(bf16[3,512]{1,0:T(4,128)(2,1)} %hidden.1, f32[2,512]{1,0:T(2,128)} %gain.1, bf16[2,64,512]{2,1,0:T(8,128)(2,1)} %bitcast.4, bf16[2,64,512]{2,1,0:T(8,128)(2,1)} %bitcast.5, bf16[2,64,512]{2,1,0:T(8,128)(2,1)} %bitcast.6, bf16[2,512,128]{2,1,0:T(8,128)(2,1)} %w_value.1, ...), custom_call_target="tpu_custom_call" | custom-call | tf_op jit(solution)/shard_map/decode/pallas_call | solution.py:447
  113.6 0.9 store_results.1

commit v7 on v6

--- a/solution.py
+++ b/solution.py
@@ -381,7 +381,11 @@
                 mine(l, k)
             else:
                 fn = {"F": forward, "A": project, "O": out_project}[step[0]]
-                for i in nearby(k):
+                order = nearby(k)
+                if l > 0 and len(order) == 2:
+                    upper = group < n_dp // 2
+                    order = [jnp.where(upper, order[1], order[0]), jnp.where(upper, order[0], order[1])]
+                for i in order:
                     fn(l, i)
 
         with jax.named_scope("owner_wait"):

time: 115 us -> 114 us (level)
  no operation moved by 1% of the time
where the time goes in v7:
time: 114 us
  Pallas kernels  113 us (99%)
    pallas_call x1, Pallas kernels, per_device(): pl.pallas_call(functools.partial(kernel, n_tp, n_dp), name='decode', out_...  113 us

profile of v7, /device:TPU:33, one launch (start us, length us, event | category | flops | bytes accessed | tf_op | source)
XLA Modules:
  0.0 114.1 jit_solution(16399683236964416589)
XLA Ops:
  0.6 112.5 %decode.1 = (bf16[3,512]{1,0:T(4,128)(2,1)S(1)}, f32[2,12,1,64,128]{4,3,2,1,0:T(8,128)S(1)}) custom-call(bf16[3,512]{1,0:T(4,128)(2,1)} %hidden.1, f32[2,512]{1,0:T(2,128)} %gain.1, bf16[2,64,512]{2,1,0:T(8,128)(2,1)} %bitcast.4, bf16[2,64,512]{2,1,0:T(8,128)(2,1)} %bitcast.5, bf16[2,64,512]{2,1,0:T(8,128)(2,1)} %bitcast.6, bf16[2,512,128]{2,1,0:T(8,128)(2,1)} %w_value.1, ...), custom_call_target="tpu_custom_call" | custom-call | tf_op jit(solution)/shard_map/decode/pallas_call | solution.py:451
  113.2 0.9 store_results.1

commit v8 on v7

--- a/solution.py
+++ b/solution.py
@@ -382,8 +382,8 @@
             else:
                 fn = {"F": forward, "A": project, "O": out_project}[step[0]]
                 order = nearby(k)
-                if l > 0 and len(order) == 2:
-                    upper = group < n_dp // 2
+                if len(order) == 2 and (l > 0 or step[0] != "F"):
+                    upper = group < n_dp // 2 if l > 0 else group >= n_dp // 2
                     order = [jnp.where(upper, order[1], order[0]), jnp.where(upper, order[0], order[1])]
                 for i in order:
                     fn(l, i)

time: 114 us -> 114 us (level)
  no operation moved by 1% of the time
where the time goes in v8:
time: 114 us; the launch traced here: 113 us
  Pallas kernels  113 us (99%)
    pallas_call x1, Pallas kernels, per_device(): pl.pallas_call(functools.partial(kernel, n_tp, n_dp), name='decode', out_...  112 us

profile of v8, /device:TPU:33, one launch (start us, length us, event | category | flops | bytes accessed | tf_op | source)
XLA Modules:
  0.0 113.4 jit_solution(5580555937788188594)
XLA Ops:
  0.6 111.9 %decode.1 = (bf16[3,512]{1,0:T(4,128)(2,1)S(1)}, f32[2,12,1,64,128]{4,3,2,1,0:T(8,128)S(1)}) custom-call(bf16[3,512]{1,0:T(4,128)(2,1)} %hidden.1, f32[2,512]{1,0:T(2,128)} %gain.1, bf16[2,64,512]{2,1,0:T(8,128)(2,1)} %bitcast.4, bf16[2,64,512]{2,1,0:T(8,128)(2,1)} %bitcast.5, bf16[2,64,512]{2,1,0:T(8,128)(2,1)} %bitcast.6, bf16[2,512,128]{2,1,0:T(8,128)(2,1)} %w_value.1, ...), custom_call_target="tpu_custom_call" | custom-call | tf_op jit(solution)/shard_map/decode/pallas_call | solution.py:451
  112.5 0.9 store_results.1
